TPU v7x, 32 devices: a whole 2x2x4 slice. The times are simulated.
32 devices in a mesh: grp: 2 (over x), ep: 16 (over z, y, core).
Axes of the slice: x: 2, y: 2, z: 4, core: 2. Of those that a mesh axis runs over, the one named last changes fastest.
Arguments:
- resid: bfloat16 [384, 2048], P(('grp', 'ep')), parts along dimension 0, may hold values from -6 to 6
- norm_gains: float32 [4, 2048], replicated, may hold values from 0.1 to 1.9
- w_query: bfloat16 [2048, 1024], P(None, 'ep'), may hold values from -0.125 to 0.125
- w_key: bfloat16 [2048, 1024], P(None, 'ep'), may hold values from -0.125 to 0.125
- w_value: bfloat16 [2048, 1024], P(None, 'ep'), may hold values from -0.125 to 0.125
- w_outgate: bfloat16 [2048, 1024], P(None, 'ep'), may hold values from -0.125 to 0.125
- w_igate: bfloat16 [2048, 8], replicated, may hold values from -0.125 to 0.125
- w_fgate: bfloat16 [2048, 8], replicated, may hold values from -0.125 to 0.125
- igate_bias: float32 [8], replicated, may hold values from -1 to 1
- fgate_bias: float32 [8], replicated, may hold values from -1 to 5
- state_matrix: float32 [384, 8, 128, 128], P(('grp', 'ep')), parts along dimension 0, may hold values from -0.8 to 0.8
- state_norm: float32 [384, 8, 128], P(('grp', 'ep')), parts along dimension 0, may hold values from -2.4 to 2.4
- state_max: float32 [384, 8], P(('grp', 'ep')), parts along dimension 0, may hold values from -1 to 1
- w_mix_out: bfloat16 [1024, 2048], replicated, may hold values from -0.1875 to 0.1875
- routes: int32 [384, 2], P(('grp', 'ep')), parts along dimension 0, may hold values from 0 to 15, all different within a row; in each aligned block of 12 rows (0 to 11, 12 to 23, ...) at most 2 rows name the same one
- route_scores: bfloat16 [384, 2], P(('grp', 'ep')), parts along dimension 0, may hold values from 0.099609375 to 1
- expert_gate: bfloat16 [16, 2048, 512], P('ep'), may hold values from -0.125 to 0.125
- expert_up: bfloat16 [16, 2048, 512], P('ep'), may hold values from -0.125 to 0.125
- expert_down: bfloat16 [16, 512, 2048], P('ep'), may hold values from -0.25 to 0.25
- dense_gate: bfloat16 [2048, 8192], P(None, 'ep'), may hold values from -0.125 to 0.125
- dense_up: bfloat16 [2048, 8192], P(None, 'ep'), may hold values from -0.125 to 0.125
- dense_down: bfloat16 [8192, 2048], P('ep'), may hold values from -0.0625 to 0.0625
- branch_weight: bfloat16 [2048], replicated, may hold values from -0.125 to 0.125
Outputs:
- out_stream: bfloat16 [384, 2048], P(('grp', 'ep')), parts along dimension 0
- new_matrix: float32 [384, 8, 128, 128], P(('grp', 'ep')), parts along dimension 0
- new_norm: float32 [384, 8, 128], P(('grp', 'ep')), parts along dimension 0
- new_max: float32 [384, 8], P(('grp', 'ep')), parts along dimension 0
There are 2 independent parts, one for each index of `grp`. A program takes and returns all parts, laid end to end along the dimension named above; an argument that names none is the same for every part. Nothing has to cross between parts.
Inputs may be any that keep to these rules, and one draw needn't show every extreme that they name: `routes`: each row names 2 different experts. In each aligned block of 12 rows (the rows of one device) no expert is named by more than 2 rows, a bound that some block reaches.
All inputs are finite; a program needn't handle non-finite values.
Results may differ from a plain program's by a relative error of at most 0.015.
Values may be sent and summed in bfloat16 or wider, within the bound.
A program may use at most 128 MiB of HBM per device.

v0:
```python
import jax
import jax.numpy as jnp
from jax import lax
from jax.sharding import PartitionSpec as P

CAP = 2


def rms_scale(values, gains):
    return values * lax.rsqrt(jnp.mean(values * values, axis=-1, keepdims=True) + 1e-06) * gains


def expert_batch(picked, gate_matrix, up_matrix, down_matrix):
    gate_out = jnp.einsum("jrd,jdf->jrf", picked, gate_matrix, preferred_element_type=jnp.float32)
    up_out = jnp.einsum("jrd,jdf->jrf", picked, up_matrix, preferred_element_type=jnp.float32)
    hidden = (jax.nn.silu(gate_out) * up_out).astype(jnp.bfloat16)
    return jnp.einsum(
        "jrf,jfd->jrd", hidden, down_matrix, preferred_element_type=jnp.float32
    ).astype(jnp.bfloat16)


def route_tables(routes, route_scores, expert_ids):
    onehot = (routes[:, :, None] == expert_ids[None, None, :]).astype(jnp.float32)
    scores = route_scores.astype(jnp.float32)
    shares = scores / jnp.sum(scores, axis=-1, keepdims=True)
    weights = jnp.sum(shares[:, :, None] * onehot, axis=1)
    hit_count = jnp.sum(onehot, axis=1)
    return (weights, hit_count)


def exchanged_experts(
    branch_in, routes, route_scores, expert_gate, expert_up, expert_down, devices_ep
):
    experts = expert_gate.shape[0] * devices_ep
    weights, hit_count = route_tables(routes, route_scores, jnp.arange(experts, dtype=jnp.int32))
    hit_int = hit_count.astype(jnp.int32)
    rank_index = jnp.cumsum(hit_int, axis=0) - hit_int
    slot_range = jnp.arange(CAP, dtype=jnp.int32)
    chosen = (
        (rank_index.T[:, None, :] == slot_range[None, :, None]) & (hit_count.T[:, None, :] > 0.5)
    ).astype(jnp.float32)
    outgoing = jnp.einsum(
        "ect,td->ecd", chosen.astype(jnp.bfloat16), branch_in, preferred_element_type=jnp.float32
    ).astype(jnp.bfloat16)
    incoming = lax.all_to_all(outgoing, "ep", split_axis=0, concat_axis=1, tiled=True)
    produced = expert_batch(incoming, expert_gate, expert_up, expert_down)
    returned = lax.all_to_all(produced, "ep", split_axis=1, concat_axis=0, tiled=True)
    weighted = chosen * weights.T[:, None, :]
    each_expert = jnp.einsum(
        "ect,ecd->etd", weighted, returned.astype(jnp.float32), precision=lax.Precision.HIGHEST
    )
    return jnp.sum(each_expert.astype(jnp.bfloat16).astype(jnp.float32), axis=0)


def local(
    resid,
    norm_gains,
    w_query,
    w_key,
    w_value,
    w_outgate,
    w_igate,
    w_fgate,
    igate_bias,
    fgate_bias,
    state_matrix,
    state_norm,
    state_max,
    w_mix_out,
    routes,
    route_scores,
    expert_gate,
    expert_up,
    expert_down,
    dense_gate,
    dense_up,
    dense_down,
    branch_weight,
):
    seqs_local = resid.shape[0]
    heads = state_matrix.shape[1]
    head_size = state_matrix.shape[2]
    devices_ep = lax.axis_size("ep")
    resid32 = resid.astype(jnp.float32)
    normed = rms_scale(resid32, norm_gains[0]).astype(jnp.bfloat16)
    row_piece = lax.all_gather(normed, "ep", axis=0, tiled=True)
    projected = jnp.stack(
        [
            jnp.dot(row_piece, matrix, preferred_element_type=jnp.float32).astype(jnp.bfloat16)
            for matrix in (w_query, w_key, w_value, w_outgate)
        ],
        axis=1,
    )
    own_proj = lax.all_to_all(projected, "ep", split_axis=0, concat_axis=2, tiled=True)
    head_shape = (seqs_local, heads, head_size)
    query = own_proj[:, 0].astype(jnp.float32).reshape(head_shape)
    key_heads = own_proj[:, 1].astype(jnp.float32).reshape(head_shape) * head_size ** (-0.5)
    value_heads = own_proj[:, 2].astype(jnp.float32).reshape(head_shape)
    outgate = own_proj[:, 3].astype(jnp.float32).reshape(head_shape)
    ipre = jnp.dot(normed, w_igate, preferred_element_type=jnp.float32) + igate_bias
    fpre = jnp.dot(normed, w_fgate, preferred_element_type=jnp.float32) + fgate_bias
    logf = jax.nn.log_sigmoid(fpre)
    new_max = jnp.maximum(ipre, logf + state_max)
    keep_gain = jnp.exp(logf + state_max - new_max)
    write_gain = jnp.exp(ipre - new_max)
    new_matrix = (
        keep_gain[:, :, None, None] * state_matrix
        + write_gain[:, :, None, None] * value_heads[:, :, :, None] * key_heads[:, :, None, :]
    )
    new_norm = keep_gain[:, :, None] * state_norm + write_gain[:, :, None] * key_heads
    numer = jnp.einsum("shed,shd->she", new_matrix, query, precision=lax.Precision.HIGHEST)
    denom = jnp.sum(new_norm * query, axis=-1)
    cell = numer / jnp.maximum(jnp.abs(denom), 1.0)[:, :, None]
    gated = (
        (jax.nn.sigmoid(outgate) * cell).reshape(seqs_local, heads * head_size).astype(jnp.bfloat16)
    )
    mixed = jnp.dot(gated, w_mix_out, preferred_element_type=jnp.float32)
    middle = resid32 + rms_scale(mixed, norm_gains[1])
    branch_in = rms_scale(middle, norm_gains[2]).astype(jnp.bfloat16)
    all_rows = lax.all_gather(branch_in, "ep", axis=0, tiled=True)
    moe_own = exchanged_experts(
        branch_in, routes, route_scores, expert_gate, expert_up, expert_down, devices_ep
    )
    gate_out = jnp.dot(all_rows, dense_gate, preferred_element_type=jnp.float32)
    up_out = jnp.dot(all_rows, dense_up, preferred_element_type=jnp.float32)
    hidden = (jax.nn.silu(gate_out) * up_out).astype(jnp.bfloat16)
    logit = jnp.dot(all_rows, branch_weight, preferred_element_type=jnp.float32)
    summed = lax.psum_scatter(
        (
            jnp.dot(hidden, dense_down, preferred_element_type=jnp.float32)
            * jax.nn.sigmoid(logit)[:, None]
        ).astype(jnp.bfloat16),
        "ep",
        scatter_dimension=0,
        tiled=True,
    ).astype(jnp.float32)
    combined = moe_own + summed
    out_stream = (middle + rms_scale(combined, norm_gains[3])).astype(jnp.bfloat16)
    return (out_stream, new_matrix, new_norm, new_max)


def solution(mesh):
    placed = (
        P(("grp", "ep"), None),
        P(),
        P(None, "ep"),
        P(None, "ep"),
        P(None, "ep"),
        P(None, "ep"),
        P(),
        P(),
        P(),
        P(),
        P(("grp", "ep"), None, None, None),
        P(("grp", "ep"), None, None),
        P(("grp", "ep"), None),
        P(),
        P(("grp", "ep"), None),
        P(("grp", "ep"), None),
        P("ep", None, None),
        P("ep", None, None),
        P("ep", None, None),
        P(None, "ep"),
        P(None, "ep"),
        P("ep", None),
        P(),
    )
    return jax.shard_map(
        local,
        mesh=mesh,
        in_specs=placed,
        out_specs=(
            P(("grp", "ep"), None),
            P(("grp", "ep"), None, None, None),
            P(("grp", "ep"), None, None),
            P(("grp", "ep"), None),
        ),
        check_vma=False,
    )
```

profile of v0, /device:TPU:17, one launch (start us, length us, event | category | flops | bytes accessed | tf_op | source)
XLA Modules:
  0.0 161.0 jit_solution(14762901746730829710)
XLA Ops:
  0.7 1.0 fusion.62
  3.6 21.5 %all-gather = bf16[16,12,2048]{2,1,0:T(8,128)(2,1)} all-gather(bf16[1,12,2048]{2,1,0:T(8,128)(2,1)S(1)} %fusion.61), channel_id=1, replica_groups=mesh['grp'=2,'ep'=16] {'ep'}, dimensions={0}, use_global_device_ids=true | all-gather | bytes 835584 | tf_op jit(solution)/shard_map/all_gather | solution.py:86
  25.1 1.3 reshape.139
  29.2 8.6 %all-to-all-start = ((bf16[16,2,1536]{2,1,0:T(2,128)(2,1)}), bf16[16,2,1536]{2,1,0:T(2,128)(2,1)S(1)}, u32[]{:S(2)}, u32[]{:S(2)}) async-start(bf16[16,2,1536]{2,1,0:T(2,128)(2,1)} %reshape.151), calls=%async_computation | async-start | bytes 196608 | tf_op jit(solution)/shard_map/all_to_all | solution.py:94
  39.2 3.3 %all-to-all-done = bf16[16,2,1536]{2,1,0:T(2,128)(2,1)S(1)} async-done(((bf16[16,2,1536]{2,1,0:T(2,128)(2,1)}), bf16[16,2,1536]{2,1,0:T(2,128)(2,1)S(1)}, u32[]{:S(2)}, u32[]{:S(2)}) %all-to-all-start) | async-done | bytes 98336 | tf_op jit(solution)/shard_map/all_to_all | solution.py:94
  44.0 4.5 %multiply_add_fusion = f32[12,8,128,128]{3,2,1,0:T(8,128)S(1)} fusion(f32[12,8,128,128]{3,2,1,0:T(8,128)} %param.33, f32[12,8,128]{2,1,0:T(8,128)S(1)} %get-tuple-element.14, f32[12,8,128]{2,1,0:T(8,128)S(1)} %get-tuple-element.21, f32[12,8]{1,0:T(8,128)S(1)} %copy.78), kind=kLoop, calls=%fused_computation | loop fusion | flops 4718592 | bytes 12681600 | tf_op jit(solution)/shard_map/add | solution.py:107
  48.5 5.0 %fusion.43 = f32[12,8,1,128]{3,2,1,0:T(1,128)S(1)} fusion(f32[12,8,128,128]{3,2,1,0:T(8,128)S(1)} %multiply_add_fusion, bf16[12,4,1024]{2,1,0:T(4,128)(2,1)S(1)} %all_to_all.32), kind=kOutput, calls=%fused_computation.61 | convolution fusion | flops 18874368 | bytes 6389760 | tf_op jit(solution)/shard_map/shed,shd->she/dot_general | solution.py:111
  54.8 22.2 %all-gather.1 = bf16[16,12,2048]{2,1,0:T(8,128)(2,1)} all-gather(bf16[1,12,2048]{2,1,0:T(8,128)(2,1)S(1)} %fusion.58), channel_id=1, replica_groups=mesh['grp'=2,'ep'=16] {'ep'}, dimensions={0}, use_global_device_ids=true | all-gather | bytes 835584 | tf_op jit(solution)/shard_map/all_gather | solution.py:120
  77.0 1.3 reshape.141
  78.3 2.9 %fusion.63 = f32[192,512]{1,0:T(8,128)} fusion(bf16[192,2048]{1,0:T(8,128)(2,1)S(1)} %reshape.141, bf16[2048,512]{1,0:T(8,128)(2,1)} %param.42), kind=kOutput, calls=%fused_computation.106 | convolution fusion | flops 402653184 | bytes 3276800 | tf_op jit(solution)/shard_map/dot_general | solution.py:124
  82.6 6.1 %all-to-all-start.1 = ((bf16[16,2,2048]{2,1,0:T(2,128)(2,1)}), bf16[16,2,2048]{2,1,0:T(2,128)(2,1)S(1)}, u32[]{:S(2)}, u32[]{:S(2)}) async-start(bf16[16,2,2048]{2,1,0:T(2,128)(2,1)} %copy.88), calls=%async_computation.1 | async-start | bytes 262144 | tf_op jit(solution)/shard_map/all_to_all | solution.py:45
  88.7 3.6 %fusion.2 = bf16[192,2048]{1,0:T(8,128)(2,1)} fusion(bf16[512,2048]{1,0:T(8,128)(2,1)S(1)} %copy-done, bf16[192,2048]{1,0:T(8,128)(2,1)S(1)} %reshape.141, bf16[2048,512]{1,0:T(8,128)(2,1)} %param.43, f32[192]{0:T(256)S(1)} %add_divide_fusion, f32[192,512]{1,0:T(8,128)} %fusion.63), kind=kOutput, calls=%fused_computation.4 | convolution fusion | flops 806682624 | bytes 6161152 | tf_op jit(solution)/shard_map/dot_general | solution.py:130
  92.3 1.8 %all-to-all-done.1 = bf16[16,2,2048]{2,1,0:T(2,128)(2,1)S(1)} async-done(((bf16[16,2,2048]{2,1,0:T(2,128)(2,1)}), bf16[16,2,2048]{2,1,0:T(2,128)(2,1)S(1)}, u32[]{:S(2)}, u32[]{:S(2)}) %all-to-all-start.1) | async-done | bytes 131104 | tf_op jit(solution)/shard_map/all_to_all | solution.py:45
  94.2 2.0 %fusion.7 = f32[32,512]{1,0:T(8,128)S(1)} fusion(bf16[32,2048]{1,0:T(8,128)(2,1)S(1)} %reshape.130, bf16[1,2048,512]{2,1,0:T(8,128)(2,1)} %param.39), kind=kOutput, calls=%fused_computation.11 | convolution fusion | flops 67108864 | bytes 2293760 | tf_op jit(solution)/shard_map/jrd,jdf->jrf/dot_general | solution.py:14
  96.2 3.2 %fusion.3 = bf16[1,32,2048]{2,1,0:T(8,128)(2,1)S(1)} fusion(bf16[1,512,2048]{2,1,0:T(8,128)(2,1)} %param.41, bf16[32,2048]{1,0:T(8,128)(2,1)S(1)} %reshape.130, bf16[1,2048,512]{2,1,0:T(8,128)(2,1)} %param.40, f32[32,512]{1,0:T(8,128)S(1)} %fusion.7), kind=kOutput, calls=%fused_computation.7 | convolution fusion | flops 134381568 | bytes 4521984 | tf_op jit(solution)/shard_map/jrf,jfd->jrd/dot_general | solution.py:17
  100.2 1.4 reduce.4
  102.3 6.0 %all-to-all-start.2 = ((bf16[16,2,2048]{2,1,0:T(2,128)(2,1)}), bf16[16,2,2048]{2,1,0:T(2,128)(2,1)S(1)}, u32[]{:S(2)}, u32[]{:S(2)}) async-start(bf16[16,2,2048]{2,1,0:T(2,128)(2,1)} %reshape.153), calls=%async_computation.2 | async-start | bytes 262144 | tf_op jit(solution)/shard_map/all_to_all | solution.py:47
  108.3 28.7 %fusion = bf16[16,2048]{1,0:T(8,128)(2,1)S(1)} fusion(bf16[192,2048]{1,0:T(8,128)(2,1)S(1)} %copy-done.4), kind=kCustom, calls=%all-reduce-scatter | all-reduce-scatter fusion | flops 524289 | bytes 852480
  137.0 2.6 %collective-permute-start = (bf16[16,2048]{1,0:T(8,128)(2,1)S(1)}, bf16[16,2048]{1,0:T(8,128)(2,1)S(1)}, u32[]{:S(2)}, u32[]{:S(2)}) collective-permute-start(bf16[16,2048]{1,0:T(8,128)(2,1)S(1)} %fusion), channel_id=1, source_target_pairs={{0,1},{1,2},{2,3},{3,4},{4,5},{5,6},{6,7},{7,8},{8,9},{9,10},{10,1... | collective-permute-start | bytes 196616
  139.6 5.4 %collective-permute-start.1 = (bf16[16,2048]{1,0:T(8,128)(2,1)S(1)}, bf16[16,2048]{1,0:T(8,128)(2,1)S(1)}, u32[]{:S(2)}, u32[]{:S(2)}) collective-permute-start(bf16[16,2048]{1,0:T(8,128)(2,1)S(1)} %fusion), channel_id=1, source_target_pairs={{0,2},{1,3},{2,4},{3,5},{4,6},{5,7},{6,8},{7,9},{8,10},{9,11},{10,... | collective-permute-start | bytes 196616
  145.0 7.3 %collective-permute-start.2 = (bf16[16,2048]{1,0:T(8,128)(2,1)S(1)}, bf16[16,2048]{1,0:T(8,128)(2,1)S(1)}, u32[]{:S(2)}, u32[]{:S(2)}) collective-permute-start(bf16[16,2048]{1,0:T(8,128)(2,1)S(1)} %fusion), channel_id=1, source_target_pairs={{0,3},{1,4},{2,5},{3,6},{4,7},{5,8},{6,9},{7,10},{8,11},{9,12},{10... | collective-permute-start | bytes 196616
  152.3 1.9 %collective-permute-start.3 = (bf16[12,2048]{1,0:T(8,128)(2,1)S(1)}, bf16[12,2048]{1,0:T(8,128)(2,1)S(1)}, u32[]{:S(2)}, u32[]{:S(2)}) collective-permute-start(bf16[12,2048]{1,0:T(8,128)(2,1)S(1)} %slice.36), channel_id=1, source_target_pairs={{0,4},{1,5},{2,6},{3,7},{4,8},{5,9},{6,10},{7,11},{8,12},{9,13},{1... | collective-permute-start | bytes 147464
  155.6 1.8 %collective-permute-done.3 = bf16[12,2048]{1,0:T(8,128)(2,1)S(1)} collective-permute-done((bf16[12,2048]{1,0:T(8,128)(2,1)S(1)}, bf16[12,2048]{1,0:T(8,128)(2,1)S(1)}, u32[]{:S(2)}, u32[]{:S(2)}) %collective-permute-start.3) | collective-permute-done | bytes 49184
  159.1 1.1 fusion.9
  (107 shorter events, 14.8 us)
Async XLA Ops:
  0.6 88.1 %copy-start = (bf16[512,2048]{1,0:T(8,128)(2,1)S(1)}, bf16[512,2048]{1,0:T(8,128)(2,1)}, u32[]{:S(2)}) copy-start(bf16[512,2048]{1,0:T(8,128)(2,1)} %param.44) | copy-start | bytes 6291460
  0.6 25.8 %copy-start.5 = (bf16[2048,64]{0,1:T(8,128)(2,1)S(1)}, bf16[2048,64]{0,1:T(8,128)(2,1)}, u32[]{:S(2)}) copy-start(bf16[2048,64]{0,1:T(8,128)(2,1)} %param.25) | copy-start | bytes 786436
  2.6 24.2 %copy-start.6 = (bf16[2048,64]{0,1:T(8,128)(2,1)S(1)}, bf16[2048,64]{0,1:T(8,128)(2,1)}, u32[]{:S(2)}) copy-start(bf16[2048,64]{0,1:T(8,128)(2,1)} %param.26) | copy-start | bytes 786436
  26.8 10.9 %copy-start.14 = (bf16[12,2]{0,1:T(2,128)(2,1)S(1)}, bf16[12,2]{0,1:T(2,128)(2,1)}, u32[]{:S(2)}) copy-start(bf16[12,2]{0,1:T(2,128)(2,1)} %param.38) | copy-start | bytes 148
  26.9 11.1 %copy-start.12 = (s32[12,2]{0,1:T(2,128)S(1)}, s32[12,2]{0,1:T(2,128)}, u32[]{:S(2)}) copy-start(s32[12,2]{0,1:T(2,128)} %param.37) | copy-start | bytes 292
  26.9 11.3 %copy-start.3 = (bf16[12,2048]{1,0:T(8,128)(2,1)S(1)}, bf16[12,2048]{1,0:T(8,128)(2,1)}, u32[]{:S(2)}) copy-start(bf16[12,2048]{1,0:T(8,128)(2,1)} %param.23) | copy-start | bytes 147460
  26.9 11.3 %copy-start.15 = (bf16[2048,8]{0,1:T(8,128)(2,1)S(1)}, bf16[2048,8]{0,1:T(8,128)(2,1)}, u32[]{:S(2)}) copy-start(bf16[2048,8]{0,1:T(8,128)(2,1)} %param.30) | copy-start | bytes 98308
  26.9 11.3 %copy-start.17 = (f32[12,8]{0,1:T(8,128)S(1)}, f32[12,8]{0,1:T(8,128)}, u32[]{:S(2)}) copy-start(f32[12,8]{0,1:T(8,128)} %param.35) | copy-start | bytes 1156
  26.9 11.3 %copy-start.18 = (f32[8]{0:T(128)S(1)}, f32[8]{0:T(128)}, u32[]{:S(2)}) copy-start(f32[8]{0:T(128)} %param.32) | copy-start | bytes 100
  26.9 11.5 %copy-start.16 = (bf16[2048,8]{0,1:T(8,128)(2,1)S(1)}, bf16[2048,8]{0,1:T(8,128)(2,1)}, u32[]{:S(2)}) copy-start(bf16[2048,8]{0,1:T(8,128)(2,1)} %param.29) | copy-start | bytes 98308
  26.9 11.5 %copy-start.19 = (f32[8]{0:T(128)S(1)}, f32[8]{0:T(128)}, u32[]{:S(2)}) copy-start(f32[8]{0:T(128)} %param.31) | copy-start | bytes 100
  27.4 11.5 %copy-start.10 = (bf16[2048]{0:T(1024)(128)(2,1)S(1)}, bf16[2048]{0:T(1024)(128)(2,1)}, u32[]{:S(2)}) copy-start(bf16[2048]{0:T(1024)(128)(2,1)} %param.45) | copy-start | bytes 12292
  27.8 15.5 %copy-start.9 = (f32[12,8,128]{2,1,0:T(8,128)S(1)}, f32[12,8,128]{2,1,0:T(8,128)}, u32[]{:S(2)}) copy-start(f32[12,8,128]{2,1,0:T(8,128)} %param.34) | copy-start | bytes 147460
  29.2 13.3 %all-to-all-start = ((bf16[16,2,1536]{2,1,0:T(2,128)(2,1)}), bf16[16,2,1536]{2,1,0:T(2,128)(2,1)S(1)}, u32[]{:S(2)}, u32[]{:S(2)}) async-start(bf16[16,2,1536]{2,1,0:T(2,128)(2,1)} %reshape.151), calls=%async_computation | async-start | bytes 196608 | tf_op jit(solution)/shard_map/all_to_all | solution.py:94
  38.6 9.8 %copy-start.11 = (f32[12,8]{0,1:T(8,128)}, f32[12,8]{0,1:T(8,128)S(1)}, u32[]{:S(2)}) copy-start(f32[12,8]{0,1:T(8,128)S(1)} %get-tuple-element.10) | copy-start | bytes 1156
  48.5 5.1 %copy-start.2 = (bf16[1024,2048]{1,0:T(8,128)(2,1)S(1)}, bf16[1024,2048]{1,0:T(8,128)(2,1)}, u32[]{:S(2)}) copy-start(bf16[1024,2048]{1,0:T(8,128)(2,1)} %param.36) | copy-start | bytes 12582916
  82.6 11.5 %all-to-all-start.1 = ((bf16[16,2,2048]{2,1,0:T(2,128)(2,1)}), bf16[16,2,2048]{2,1,0:T(2,128)(2,1)S(1)}, u32[]{:S(2)}, u32[]{:S(2)}) async-start(bf16[16,2,2048]{2,1,0:T(2,128)(2,1)} %copy.88), calls=%async_computation.1 | async-start | bytes 262144 | tf_op jit(solution)/shard_map/all_to_all | solution.py:45
  96.2 12.1 %copy-start.4 = (bf16[192,2048]{1,0:T(8,128)(2,1)S(1)}, bf16[192,2048]{1,0:T(8,128)(2,1)}, u32[]{:S(2)}) copy-start(bf16[192,2048]{1,0:T(8,128)(2,1)} %fusion.2) | copy-start | bytes 2359300
  99.4 54.9 %copy-start.13 = (u32[32]{0:T(128)S(1)}, u32[32]{0:T(128)}, u32[]{:S(2)}) copy-start(u32[32]{0:T(128)} %constant.42) | copy-start | bytes 388
  102.3 55.8 %all-to-all-start.2 = ((bf16[16,2,2048]{2,1,0:T(2,128)(2,1)}), bf16[16,2,2048]{2,1,0:T(2,128)(2,1)S(1)}, u32[]{:S(2)}, u32[]{:S(2)}) async-start(bf16[16,2,2048]{2,1,0:T(2,128)(2,1)} %reshape.153), calls=%async_computation.2 | async-start | bytes 262144 | tf_op jit(solution)/shard_map/all_to_all | solution.py:47
  137.0 20.4 %collective-permute-start = (bf16[16,2048]{1,0:T(8,128)(2,1)S(1)}, bf16[16,2048]{1,0:T(8,128)(2,1)S(1)}, u32[]{:S(2)}, u32[]{:S(2)}) collective-permute-start(bf16[16,2048]{1,0:T(8,128)(2,1)S(1)} %fusion), channel_id=1, source_target_pairs={{0,1},{1,2},{2,3},{3,4},{4,5},{5,6},{6,7},{7,8},{8,9},{9,10},{10,1... | collective-permute-start | bytes 196616
  139.6 17.7 %collective-permute-start.1 = (bf16[16,2048]{1,0:T(8,128)(2,1)S(1)}, bf16[16,2048]{1,0:T(8,128)(2,1)S(1)}, u32[]{:S(2)}, u32[]{:S(2)}) collective-permute-start(bf16[16,2048]{1,0:T(8,128)(2,1)S(1)} %fusion), channel_id=1, source_target_pairs={{0,2},{1,3},{2,4},{3,5},{4,6},{5,7},{6,8},{7,9},{8,10},{9,11},{10,... | collective-permute-start | bytes 196616
  145.0 12.3 %collective-permute-start.2 = (bf16[16,2048]{1,0:T(8,128)(2,1)S(1)}, bf16[16,2048]{1,0:T(8,128)(2,1)S(1)}, u32[]{:S(2)}, u32[]{:S(2)}) collective-permute-start(bf16[16,2048]{1,0:T(8,128)(2,1)S(1)} %fusion), channel_id=1, source_target_pairs={{0,3},{1,4},{2,5},{3,6},{4,7},{5,8},{6,9},{7,10},{8,11},{9,12},{10... | collective-permute-start | bytes 196616
  152.3 5.0 %collective-permute-start.3 = (bf16[12,2048]{1,0:T(8,128)(2,1)S(1)}, bf16[12,2048]{1,0:T(8,128)(2,1)S(1)}, u32[]{:S(2)}, u32[]{:S(2)}) collective-permute-start(bf16[12,2048]{1,0:T(8,128)(2,1)S(1)} %slice.36), channel_id=1, source_target_pairs={{0,4},{1,5},{2,6},{3,7},{4,8},{5,9},{6,10},{7,11},{8,12},{9,13},{1... | collective-permute-start | bytes 147464
  (3 other events, 7.3 us)
where the time goes:
time: 162 us; the launch traced here: 161 us
  blocking collectives  72.4 us (45%)
  starting transfers between devices  37.8 us (23%)
  matrix products  21.1 us (13%)
  local copies, waits for them, and re-layouts  10.5 us (6%)
  other arithmetic  10.4 us (6%)
  waiting for transfers between devices  6.9 us (4%)
  between operations  1.84 us (1%)
    unnamed x1, blocking collectives  28.7 us
    all_gather x1, blocking collectives, local(): all_rows = lax.all_gather(branch_in, 'ep', axis=0, tiled=True)  22.2 us
    all_gather x1, blocking collectives, local(): row_piece = lax.all_gather(normed, 'ep', axis=0, tiled=True)  21.5 us
    unnamed x4, starting transfers between devices  17.2 us
    all_to_all x1, starting transfers between devices, local(): lax.all_to_all(projected, 'ep', split_axis=0, concat_axis=2, tiled=True)  8.56 us
    unnamed x55, local copies, waits for them, and re-layouts  6.65 us
    all_to_all x1, starting transfers between devices, exchanged_experts(): lax.all_to_all(outgoing, 'ep', split_axis=0, concat_axis=1, tiled=True)  6.08 us
    all_to_all x1, starting transfers between devices, exchanged_experts(): lax.all_to_all(produced, 'ep', split_axis=1, concat_axis=0, tiled=True)  5.97 us
  transfers between devices with their start and end apart: 7, of which 3 were waited for; matrix products, arithmetic and copies ran while one was open for 22% of the time, Pallas kernels for 0%

commit v1 on v0

--- a/solution.py
+++ b/solution.py
@@ -117,7 +117,12 @@
     mixed = jnp.dot(gated, w_mix_out, preferred_element_type=jnp.float32)
     middle = resid32 + rms_scale(mixed, norm_gains[1])
     branch_in = rms_scale(middle, norm_gains[2]).astype(jnp.bfloat16)
-    all_rows = lax.all_gather(branch_in, "ep", axis=0, tiled=True)
+    ring = [branch_in]
+    for hop in range(15):
+        ring.append(lax.ppermute(ring[-1], "ep", [(dev, (dev + 1) % 16) for dev in range(16)]))
+    all_rows = jnp.roll(
+        jnp.concatenate(ring[::-1], axis=0), (lax.axis_index("ep") + 1) * ring[0].shape[0], axis=0
+    )
     moe_own = exchanged_experts(
         branch_in, routes, route_scores, expert_gate, expert_up, expert_down, devices_ep
     )

time: 162 us -> 254 us (1.57)
  starting transfers between devices: 37.8 us -> 85.9 us
  local copies, waits for them, and re-layouts: 10.5 us -> 51.7 us
  waiting for transfers between devices: 6.9 us -> 26.3 us
  blocking collectives: 72.4 us -> 54.1 us
    concatenate x0 -> x1, local copies, waits for them, and re-layouts: none -> 37.9 us  [local(): jnp.roll(jnp.concatenate(ring[::-1], axis=0), (lax.axis_index('ep') + 1)...]
    ppermute x0 -> x15, starting transfers between devices: none -> 25.1 us  [local(): lax.ppermute(ring[-1], 'ep', [(dev, (dev + 1) % 16) for dev in range(16)])]
    all_gather x1 -> x0, blocking collectives: 22.2 us -> none  [local(): all_rows = lax.all_gather(branch_in, 'ep', axis=0, tiled=True)]
    ppermute x0 -> x15, waiting for transfers between devices: none -> 21.3 us  [local(): lax.ppermute(ring[-1], 'ep', [(dev, (dev + 1) % 16) for dev in range(16)])]
    all_to_all x1, starting transfers between devices: 5.97 us -> 16.7 us  [exchanged_experts(): lax.all_to_all(produced, 'ep', split_axis=1, concat_axis=0, tiled=True)]
    all_to_all x1, starting transfers between devices: 6.08 us -> 13.3 us  [exchanged_experts(): lax.all_to_all(outgoing, 'ep', split_axis=0, concat_axis=1, tiled=True)]
    unnamed x4, starting transfers between devices: 17.2 us -> 22.2 us
    unnamed x1, blocking collectives: 28.7 us -> 32.6 us
  transfers between devices with their start and end apart: 7 -> 22, of which waited for: 3 -> 13; matrix products, arithmetic and copies ran while one was open for 22% -> 6% of each run, Pallas kernels for 0% -> 0%
where the time goes in v1:
time: 254 us; the launch traced here: 252 us
  starting transfers between devices  85.9 us (34%)
  blocking collectives  54.1 us (21%)
  local copies, waits for them, and re-layouts  51.7 us (20%)
  waiting for transfers between devices  26.3 us (10%)
  matrix products  20.9 us (8%)
  other arithmetic  11.1 us (4%)
    concatenate x1, local copies, waits for them, and re-layouts, local(): jnp.roll(jnp.concatenate(ring[::-1], axis=0), (lax.axis_index('ep') + 1)...  37.9 us
    unnamed x1, blocking collectives  32.6 us
    ppermute x15, starting transfers between devices, local(): lax.ppermute(ring[-1], 'ep', [(dev, (dev + 1) % 16) for dev in range(16)])  25.1 us
    unnamed x4, starting transfers between devices  22.2 us
    all_gather x1, blocking collectives, local(): row_piece = lax.all_gather(normed, 'ep', axis=0, tiled=True)  21.5 us
    ppermute x15, waiting for transfers between devices, local(): lax.ppermute(ring[-1], 'ep', [(dev, (dev + 1) % 16) for dev in range(16)])  21.3 us
    all_to_all x1, starting transfers between devices, exchanged_experts(): lax.all_to_all(produced, 'ep', split_axis=1, concat_axis=0, tiled=True)  16.7 us
    all_to_all x1, starting transfers between devices, exchanged_experts(): lax.all_to_all(outgoing, 'ep', split_axis=0, concat_axis=1, tiled=True)  13.3 us
  transfers between devices with their start and end apart: 22, of which 13 were waited for; matrix products, arithmetic and copies ran while one was open for 6% of the time, Pallas kernels for 0%

profile of v1, /device:TPU:17, one launch (start us, length us, event | category | flops | bytes accessed | tf_op | source)
XLA Modules:
  0.0 251.8 jit_solution(8267765139773000615)
XLA Ops:
  4.2 21.5 %all-gather = bf16[16,12,2048]{2,1,0:T(8,128)(2,1)} all-gather(bf16[1,12,2048]{2,1,0:T(8,128)(2,1)S(1)} %fusion.68), channel_id=1, replica_groups=mesh['grp'=2,'ep'=16] {'ep'}, dimensions={0}, use_global_device_ids=true | all-gather | bytes 835584 | tf_op jit(solution)/shard_map/all_gather | solution.py:86
  29.8 8.6 %all-to-all-start = ((bf16[16,2,1536]{2,1,0:T(2,128)(2,1)}), bf16[16,2,1536]{2,1,0:T(2,128)(2,1)S(1)}, u32[]{:S(2)}, u32[]{:S(2)}) async-start(bf16[16,2,1536]{2,1,0:T(2,128)(2,1)} %reshape.149), calls=%async_computation | async-start | bytes 196608 | tf_op jit(solution)/shard_map/all_to_all | solution.py:94
  40.8 2.3 all-to-all-done
  44.6 4.5 %multiply_add_fusion = f32[12,8,128,128]{3,2,1,0:T(8,128)S(1)} fusion(f32[12,8,128,128]{3,2,1,0:T(8,128)} %param.33, f32[12,8,128]{2,1,0:T(8,128)S(1)} %get-tuple-element.14, f32[12,8,128]{2,1,0:T(8,128)S(1)} %get-tuple-element.21, f32[12,8]{1,0:T(8,128)S(1)} %copy.78), kind=kLoop, calls=%fused_computation | loop fusion | flops 4718592 | bytes 12681600 | tf_op jit(solution)/shard_map/add | solution.py:107
  49.1 5.0 %fusion.47 = f32[12,8,1,128]{3,2,1,0:T(1,128)S(1)} fusion(f32[12,8,128,128]{3,2,1,0:T(8,128)S(1)} %multiply_add_fusion, bf16[12,4,1024]{2,1,0:T(4,128)(2,1)S(1)} %all_to_all.32), kind=kOutput, calls=%fused_computation.61 | convolution fusion | flops 18874368 | bytes 6389760 | tf_op jit(solution)/shard_map/shed,shd->she/dot_general | solution.py:111
  57.3 2.4 collective-permute-start.1
  64.2 13.3 %all-to-all-start.1 = ((bf16[16,2,2048]{2,1,0:T(2,128)(2,1)}), bf16[16,2,2048]{2,1,0:T(2,128)(2,1)S(1)}, u32[]{:S(2)}, u32[]{:S(2)}) async-start(bf16[16,2,2048]{2,1,0:T(2,128)(2,1)} %copy.88), calls=%async_computation.1 | async-start | bytes 262144 | tf_op jit(solution)/shard_map/all_to_all | solution.py:45
  80.5 2.8 %collective-permute-start.4 = (bf16[12,2048]{1,0:T(8,128)(2,1)S(1)}, bf16[12,2048]{1,0:T(8,128)(2,1)S(1)}, u32[]{:S(2)}, u32[]{:S(2)}) collective-permute-start(bf16[12,2048]{1,0:T(8,128)(2,1)S(1)} %collective-permute-done.3), channel_id=1, source_target_pairs={{0,1},{1,2},{2,3},{3,4},{4,5},{5,6},{6,7},{7,8},{8,9},{9,10},{10,1... | collective-permute-start | bytes 147464 | tf_op jit(solution)/shard_map/ppermute | solution.py:122
  87.0 2.5 collective-permute-done.5
  90.7 3.3 %collective-permute-done.6 = bf16[12,2048]{1,0:T(8,128)(2,1)S(1)} collective-permute-done((bf16[12,2048]{1,0:T(8,128)(2,1)S(1)}, bf16[12,2048]{1,0:T(8,128)(2,1)S(1)}, u32[]{:S(2)}, u32[]{:S(2)}) %collective-permute-start.6) | collective-permute-done | bytes 49184 | tf_op jit(solution)/shard_map/ppermute | solution.py:122
  96.4 2.3 collective-permute-done.7
  98.6 3.1 %fusion.3 = bf16[1,32,2048]{2,1,0:T(8,128)(2,1)S(1)} fusion(bf16[1,512,2048]{2,1,0:T(8,128)(2,1)} %param.41, bf16[32,2048]{1,0:T(8,128)(2,1)S(1)} %reshape.130, bf16[1,2048,512]{2,1,0:T(8,128)(2,1)} %param.40, f32[32,512]{1,0:T(8,128)S(1)} %fusion.7), kind=kOutput, calls=%fused_computation.7 | convolution fusion | flops 134381568 | bytes 4521984 | tf_op jit(solution)/shard_map/jrf,jfd->jrd/dot_general | solution.py:17
  104.0 3.2 %collective-permute-start.9 = (bf16[12,2048]{1,0:T(8,128)(2,1)S(1)}, bf16[12,2048]{1,0:T(8,128)(2,1)S(1)}, u32[]{:S(2)}, u32[]{:S(2)}) collective-permute-start(bf16[12,2048]{1,0:T(8,128)(2,1)S(1)} %collective-permute-done.8), channel_id=1, source_target_pairs={{0,1},{1,2},{2,3},{3,4},{4,5},{5,6},{6,7},{7,8},{8,9},{9,10},{10,1... | collective-permute-start | bytes 147464 | tf_op jit(solution)/shard_map/ppermute | solution.py:122
  107.9 16.7 %all-to-all-start.2 = ((bf16[16,2,2048]{2,1,0:T(2,128)(2,1)}), bf16[16,2,2048]{2,1,0:T(2,128)(2,1)S(1)}, u32[]{:S(2)}, u32[]{:S(2)}) async-start(bf16[16,2,2048]{2,1,0:T(2,128)(2,1)} %reshape.151), calls=%async_computation.2 | async-start | bytes 262144 | tf_op jit(solution)/shard_map/all_to_all | solution.py:47
  127.6 2.8 %collective-permute-start.11 = (bf16[12,2048]{1,0:T(8,128)(2,1)S(1)}, bf16[12,2048]{1,0:T(8,128)(2,1)S(1)}, u32[]{:S(2)}, u32[]{:S(2)}) collective-permute-start(bf16[12,2048]{1,0:T(8,128)(2,1)S(1)} %collective-permute-done.10), channel_id=1, source_target_pairs={{0,1},{1,2},{2,3},{3,4},{4,5},{5,6},{6,7},{7,8},{8,9},{9,10},{10,1... | collective-permute-start | bytes 147464 | tf_op jit(solution)/shard_map/ppermute | solution.py:122
  134.1 2.6 %collective-permute-done.12 = bf16[12,2048]{1,0:T(8,128)(2,1)} collective-permute-done((bf16[12,2048]{1,0:T(8,128)(2,1)S(1)}, bf16[12,2048]{1,0:T(8,128)(2,1)}, u32[]{:S(2)}, u32[]{:S(2)}) %collective-permute-start.12) | collective-permute-done | bytes 49184 | tf_op jit(solution)/shard_map/ppermute | solution.py:122
  146.5 37.9 %concatenate.6 = bf16[384,2048]{1,0:T(8,128)(2,1)} concatenate(bf16[12,2048]{1,0:T(8,128)(2,1)} %collective-permute-done.14, bf16[12,2048]{1,0:T(8,128)(2,1)} %collective-permute-done.13, bf16[12,2048]{1,0:T(8,128)(2,1)} %collective-permute-done.12, bf16[12,2048]{1,0:T(8,128)(2,1)S(1)} %collective-permute-done.11, bf16[12,2048]{1,0:T(8,128)(2,1)S(1)} %collective-permute-done.10, ...), dimensions={0} | concatenate | bytes 3145728 | tf_op jit(solution)/shard_map/jit(_roll_dynamic)/concatenate | solution.py:123
  184.5 2.5 %fusion.25 = f32[192,512]{1,0:T(8,128)S(1)} fusion(bf16[2048,512]{1,0:T(8,128)(2,1)} %param.43, bf16[384,2048]{1,0:T(8,128)(2,1)} %concatenate.6, s32[]{:T(128)S(6)} %select_n.20), kind=kOutput, calls=%fused_computation.29 | convolution fusion | flops 402653184 | bytes 3276804 | tf_op jit(solution)/shard_map/dot_general | solution.py:130
  187.4 3.9 %fusion.2 = bf16[192,2048]{1,0:T(8,128)(2,1)} fusion(bf16[512,2048]{1,0:T(8,128)(2,1)S(1)} %copy-done, f32[192]{0:T(256)S(1)} %add_divide_fusion, f32[192,512]{1,0:T(8,128)S(1)} %fusion.25, bf16[2048,512]{1,0:T(8,128)(2,1)} %param.42, bf16[384,2048]{1,0:T(8,128)(2,1)} %concatenate.6, s32[]{:T(128)S(6)} %select_n.20), kind=kOutput, calls=%fused_computation.4 | convolution fusion | flops 806682624 | bytes 6161156 | tf_op jit(solution)/shard_map/dot_general | solution.py:135
  191.3 32.6 %fusion = bf16[16,2048]{1,0:T(8,128)(2,1)S(1)} fusion(bf16[192,2048]{1,0:T(8,128)(2,1)} %fusion.2), kind=kCustom, calls=%all-reduce-scatter | all-reduce-scatter fusion | flops 524289 | bytes 852480
  224.0 5.3 %collective-permute-start.15 = (bf16[16,2048]{1,0:T(8,128)(2,1)S(1)}, bf16[16,2048]{1,0:T(8,128)(2,1)S(1)}, u32[]{:S(2)}, u32[]{:S(2)}) collective-permute-start(bf16[16,2048]{1,0:T(8,128)(2,1)S(1)} %fusion), channel_id=1, source_target_pairs={{0,1},{1,2},{2,3},{3,4},{4,5},{5,6},{6,7},{7,8},{8,9},{9,10},{10,1... | collective-permute-start | bytes 196616
  229.3 7.5 %collective-permute-start.16 = (bf16[16,2048]{1,0:T(8,128)(2,1)S(1)}, bf16[16,2048]{1,0:T(8,128)(2,1)S(1)}, u32[]{:S(2)}, u32[]{:S(2)}) collective-permute-start(bf16[16,2048]{1,0:T(8,128)(2,1)S(1)} %fusion), channel_id=1, source_target_pairs={{0,2},{1,3},{2,4},{3,5},{4,6},{5,7},{6,8},{7,9},{8,10},{9,11},{10,... | collective-permute-start | bytes 196616
  236.8 7.5 %collective-permute-start.17 = (bf16[16,2048]{1,0:T(8,128)(2,1)S(1)}, bf16[16,2048]{1,0:T(8,128)(2,1)S(1)}, u32[]{:S(2)}, u32[]{:S(2)}) collective-permute-start(bf16[16,2048]{1,0:T(8,128)(2,1)S(1)} %fusion), channel_id=1, source_target_pairs={{0,3},{1,4},{2,5},{3,6},{4,7},{5,8},{6,9},{7,10},{8,11},{9,12},{10... | collective-permute-start | bytes 196616
  247.4 2.7 %collective-permute-done.18 = bf16[12,2048]{1,0:T(8,128)(2,1)S(1)} collective-permute-done((bf16[12,2048]{1,0:T(8,128)(2,1)S(1)}, bf16[12,2048]{1,0:T(8,128)(2,1)S(1)}, u32[]{:S(2)}, u32[]{:S(2)}) %collective-permute-start.18) | collective-permute-done | bytes 49184
  (150 shorter events, 53.1 us)
Async XLA Ops:
  0.6 186.7 %copy-start = (bf16[512,2048]{1,0:T(8,128)(2,1)S(1)}, bf16[512,2048]{1,0:T(8,128)(2,1)}, u32[]{:S(2)}) copy-start(bf16[512,2048]{1,0:T(8,128)(2,1)} %param.44) | copy-start | bytes 6291460
  29.8 13.3 %all-to-all-start = ((bf16[16,2,1536]{2,1,0:T(2,128)(2,1)}), bf16[16,2,1536]{2,1,0:T(2,128)(2,1)S(1)}, u32[]{:S(2)}, u32[]{:S(2)}) async-start(bf16[16,2,1536]{2,1,0:T(2,128)(2,1)} %reshape.149), calls=%async_computation | async-start | bytes 196608 | tf_op jit(solution)/shard_map/all_to_all | solution.py:94
  55.3 2.0 collective-permute-start
  57.3 3.8 %collective-permute-start.1 = (bf16[12,2048]{1,0:T(8,128)(2,1)S(1)}, bf16[12,2048]{1,0:T(8,128)(2,1)S(1)}, u32[]{:S(2)}, u32[]{:S(2)}) collective-permute-start(bf16[12,2048]{1,0:T(8,128)(2,1)S(1)} %collective-permute-done), channel_id=1, source_target_pairs={{0,1},{1,2},{2,3},{3,4},{4,5},{5,6},{6,7},{7,8},{8,9},{9,10},{10,1... | collective-permute-start | bytes 147464 | tf_op jit(solution)/shard_map/ppermute | solution.py:122
  61.1 16.4 %collective-permute-start.2 = (bf16[12,2048]{1,0:T(8,128)(2,1)S(1)}, bf16[12,2048]{1,0:T(8,128)(2,1)S(1)}, u32[]{:S(2)}, u32[]{:S(2)}) collective-permute-start(bf16[12,2048]{1,0:T(8,128)(2,1)S(1)} %collective-permute-done.1), channel_id=1, source_target_pairs={{0,1},{1,2},{2,3},{3,4},{4,5},{5,6},{6,7},{7,8},{8,9},{9,10},{10,1... | collective-permute-start | bytes 147464 | tf_op jit(solution)/shard_map/ppermute | solution.py:122
  64.2 26.5 %all-to-all-start.1 = ((bf16[16,2,2048]{2,1,0:T(2,128)(2,1)}), bf16[16,2,2048]{2,1,0:T(2,128)(2,1)S(1)}, u32[]{:S(2)}, u32[]{:S(2)}) async-start(bf16[16,2,2048]{2,1,0:T(2,128)(2,1)} %copy.88), calls=%async_computation.1 | async-start | bytes 262144 | tf_op jit(solution)/shard_map/all_to_all | solution.py:45
  77.5 3.0 %collective-permute-start.3 = (bf16[12,2048]{1,0:T(8,128)(2,1)S(1)}, bf16[12,2048]{1,0:T(8,128)(2,1)S(1)}, u32[]{:S(2)}, u32[]{:S(2)}) collective-permute-start(bf16[12,2048]{1,0:T(8,128)(2,1)S(1)} %collective-permute-done.2), channel_id=1, source_target_pairs={{0,1},{1,2},{2,3},{3,4},{4,5},{5,6},{6,7},{7,8},{8,9},{9,10},{10,1... | collective-permute-start | bytes 147464 | tf_op jit(solution)/shard_map/ppermute | solution.py:122
  80.5 4.4 %collective-permute-start.4 = (bf16[12,2048]{1,0:T(8,128)(2,1)S(1)}, bf16[12,2048]{1,0:T(8,128)(2,1)S(1)}, u32[]{:S(2)}, u32[]{:S(2)}) collective-permute-start(bf16[12,2048]{1,0:T(8,128)(2,1)S(1)} %collective-permute-done.3), channel_id=1, source_target_pairs={{0,1},{1,2},{2,3},{3,4},{4,5},{5,6},{6,7},{7,8},{8,9},{9,10},{10,1... | collective-permute-start | bytes 147464 | tf_op jit(solution)/shard_map/ppermute | solution.py:122
  84.9 4.6 %collective-permute-start.5 = (bf16[12,2048]{1,0:T(8,128)(2,1)S(1)}, bf16[12,2048]{1,0:T(8,128)(2,1)S(1)}, u32[]{:S(2)}, u32[]{:S(2)}) collective-permute-start(bf16[12,2048]{1,0:T(8,128)(2,1)S(1)} %collective-permute-done.4), channel_id=1, source_target_pairs={{0,1},{1,2},{2,3},{3,4},{4,5},{5,6},{6,7},{7,8},{8,9},{9,10},{10,1... | collective-permute-start | bytes 147464 | tf_op jit(solution)/shard_map/ppermute | solution.py:122
  89.4 4.6 %collective-permute-start.6 = (bf16[12,2048]{1,0:T(8,128)(2,1)S(1)}, bf16[12,2048]{1,0:T(8,128)(2,1)S(1)}, u32[]{:S(2)}, u32[]{:S(2)}) collective-permute-start(bf16[12,2048]{1,0:T(8,128)(2,1)S(1)} %collective-permute-done.5), channel_id=1, source_target_pairs={{0,1},{1,2},{2,3},{3,4},{4,5},{5,6},{6,7},{7,8},{8,9},{9,10},{10,1... | collective-permute-start | bytes 147464 | tf_op jit(solution)/shard_map/ppermute | solution.py:122
  94.0 4.6 %collective-permute-start.7 = (bf16[12,2048]{1,0:T(8,128)(2,1)S(1)}, bf16[12,2048]{1,0:T(8,128)(2,1)S(1)}, u32[]{:S(2)}, u32[]{:S(2)}) collective-permute-start(bf16[12,2048]{1,0:T(8,128)(2,1)S(1)} %collective-permute-done.6), channel_id=1, source_target_pairs={{0,1},{1,2},{2,3},{3,4},{4,5},{5,6},{6,7},{7,8},{8,9},{9,10},{10,1... | collective-permute-start | bytes 147464 | tf_op jit(solution)/shard_map/ppermute | solution.py:122
  98.6 5.4 %collective-permute-start.8 = (bf16[12,2048]{1,0:T(8,128)(2,1)S(1)}, bf16[12,2048]{1,0:T(8,128)(2,1)S(1)}, u32[]{:S(2)}, u32[]{:S(2)}) collective-permute-start(bf16[12,2048]{1,0:T(8,128)(2,1)S(1)} %collective-permute-done.7), channel_id=1, source_target_pairs={{0,1},{1,2},{2,3},{3,4},{4,5},{5,6},{6,7},{7,8},{8,9},{9,10},{10,1... | collective-permute-start | bytes 147464 | tf_op jit(solution)/shard_map/ppermute | solution.py:122
  104.0 20.6 %collective-permute-start.9 = (bf16[12,2048]{1,0:T(8,128)(2,1)S(1)}, bf16[12,2048]{1,0:T(8,128)(2,1)S(1)}, u32[]{:S(2)}, u32[]{:S(2)}) collective-permute-start(bf16[12,2048]{1,0:T(8,128)(2,1)S(1)} %collective-permute-done.8), channel_id=1, source_target_pairs={{0,1},{1,2},{2,3},{3,4},{4,5},{5,6},{6,7},{7,8},{8,9},{9,10},{10,1... | collective-permute-start | bytes 147464 | tf_op jit(solution)/shard_map/ppermute | solution.py:122
  107.9 33.9 %all-to-all-start.2 = ((bf16[16,2,2048]{2,1,0:T(2,128)(2,1)}), bf16[16,2,2048]{2,1,0:T(2,128)(2,1)S(1)}, u32[]{:S(2)}, u32[]{:S(2)}) async-start(bf16[16,2,2048]{2,1,0:T(2,128)(2,1)} %reshape.151), calls=%async_computation.2 | async-start | bytes 262144 | tf_op jit(solution)/shard_map/all_to_all | solution.py:47
  124.6 3.0 %collective-permute-start.10 = (bf16[12,2048]{1,0:T(8,128)(2,1)S(1)}, bf16[12,2048]{1,0:T(8,128)(2,1)S(1)}, u32[]{:S(2)}, u32[]{:S(2)}) collective-permute-start(bf16[12,2048]{1,0:T(8,128)(2,1)S(1)} %collective-permute-done.9), channel_id=1, source_target_pairs={{0,1},{1,2},{2,3},{3,4},{4,5},{5,6},{6,7},{7,8},{8,9},{9,10},{10,1... | collective-permute-start | bytes 147464 | tf_op jit(solution)/shard_map/ppermute | solution.py:122
  127.6 4.4 %collective-permute-start.11 = (bf16[12,2048]{1,0:T(8,128)(2,1)S(1)}, bf16[12,2048]{1,0:T(8,128)(2,1)S(1)}, u32[]{:S(2)}, u32[]{:S(2)}) collective-permute-start(bf16[12,2048]{1,0:T(8,128)(2,1)S(1)} %collective-permute-done.10), channel_id=1, source_target_pairs={{0,1},{1,2},{2,3},{3,4},{4,5},{5,6},{6,7},{7,8},{8,9},{9,10},{10,1... | collective-permute-start | bytes 147464 | tf_op jit(solution)/shard_map/ppermute | solution.py:122
  132.0 4.7 %collective-permute-start.12 = (bf16[12,2048]{1,0:T(8,128)(2,1)S(1)}, bf16[12,2048]{1,0:T(8,128)(2,1)}, u32[]{:S(2)}, u32[]{:S(2)}) collective-permute-start(bf16[12,2048]{1,0:T(8,128)(2,1)S(1)} %collective-permute-done.11), channel_id=1, source_target_pairs={{0,1},{1,2},{2,3},{3,4},{4,5},{5,6},{6,7},{7,8},{8,9},{9,10},{10,1... | collective-permute-start | bytes 147464 | tf_op jit(solution)/shard_map/ppermute | solution.py:122
  136.7 5.3 %collective-permute-start.13 = (bf16[12,2048]{1,0:T(8,128)(2,1)}, bf16[12,2048]{1,0:T(8,128)(2,1)}, u32[]{:S(2)}, u32[]{:S(2)}) collective-permute-start(bf16[12,2048]{1,0:T(8,128)(2,1)} %collective-permute-done.12), channel_id=1, source_target_pairs={{0,1},{1,2},{2,3},{3,4},{4,5},{5,6},{6,7},{7,8},{8,9},{9,10},{10,1... | collective-permute-start | bytes 147464 | tf_op jit(solution)/shard_map/ppermute | solution.py:122
  142.0 4.5 %collective-permute-start.14 = (bf16[12,2048]{1,0:T(8,128)(2,1)}, bf16[12,2048]{1,0:T(8,128)(2,1)}, u32[]{:S(2)}, u32[]{:S(2)}) collective-permute-start(bf16[12,2048]{1,0:T(8,128)(2,1)} %collective-permute-done.13), channel_id=1, source_target_pairs={{0,1},{1,2},{2,3},{3,4},{4,5},{5,6},{6,7},{7,8},{8,9},{9,10},{10,1... | collective-permute-start | bytes 147464 | tf_op jit(solution)/shard_map/ppermute | solution.py:122
  191.3 59.7 %copy-start.18 = (f32[12]{0:T(128)S(1)}, f32[12]{0:T(128)}, u32[]{:S(2)}) copy-start(f32[12]{0:T(128)} %copy-done.17) | copy-start | bytes 148
  224.0 26.1 %collective-permute-start.15 = (bf16[16,2048]{1,0:T(8,128)(2,1)S(1)}, bf16[16,2048]{1,0:T(8,128)(2,1)S(1)}, u32[]{:S(2)}, u32[]{:S(2)}) collective-permute-start(bf16[16,2048]{1,0:T(8,128)(2,1)S(1)} %fusion), channel_id=1, source_target_pairs={{0,1},{1,2},{2,3},{3,4},{4,5},{5,6},{6,7},{7,8},{8,9},{9,10},{10,1... | collective-permute-start | bytes 196616
  229.3 20.8 %collective-permute-start.16 = (bf16[16,2048]{1,0:T(8,128)(2,1)S(1)}, bf16[16,2048]{1,0:T(8,128)(2,1)S(1)}, u32[]{:S(2)}, u32[]{:S(2)}) collective-permute-start(bf16[16,2048]{1,0:T(8,128)(2,1)S(1)} %fusion), channel_id=1, source_target_pairs={{0,2},{1,3},{2,4},{3,5},{4,6},{5,7},{6,8},{7,9},{8,10},{9,11},{10,... | collective-permute-start | bytes 196616
  236.8 13.3 %collective-permute-start.17 = (bf16[16,2048]{1,0:T(8,128)(2,1)S(1)}, bf16[16,2048]{1,0:T(8,128)(2,1)S(1)}, u32[]{:S(2)}, u32[]{:S(2)}) collective-permute-start(bf16[16,2048]{1,0:T(8,128)(2,1)S(1)} %fusion), channel_id=1, source_target_pairs={{0,3},{1,4},{2,5},{3,6},{4,7},{5,8},{6,9},{7,10},{8,11},{9,12},{10... | collective-permute-start | bytes 196616
  244.3 5.7 %collective-permute-start.18 = (bf16[12,2048]{1,0:T(8,128)(2,1)S(1)}, bf16[12,2048]{1,0:T(8,128)(2,1)S(1)}, u32[]{:S(2)}, u32[]{:S(2)}) collective-permute-start(bf16[12,2048]{1,0:T(8,128)(2,1)S(1)} %slice.36), channel_id=1, source_target_pairs={{0,4},{1,5},{2,6},{3,7},{4,8},{5,9},{6,10},{7,11},{8,12},{9,13},{1... | collective-permute-start | bytes 147464
  (25 other events, 498.0 us)
